TPU v7x, 32 devices: a whole 2x2x4 slice. The times are simulated.
32 devices in a mesh: sp: 8 (over z, y), tp: 4 (over x, core).
Axes of the slice: x: 2, y: 2, z: 4, core: 2. Of those that a mesh axis runs over, the one named last changes fastest.
Arguments:
- tokens: bfloat16 [2048, 4096], P(('sp', 'tp')), may hold values from -6 to 6, as said below
- query_one: bfloat16 [4096, 1024], P('sp', 'tp'), may hold values from -0.125 to 0.125
- query_two: bfloat16 [4096, 1024], P('sp', 'tp'), may hold values from -0.125 to 0.125
- key_one: bfloat16 [4096, 1024], P('sp', 'tp'), may hold values from -0.125 to 0.125
- key_two: bfloat16 [4096, 1024], P('sp', 'tp'), may hold values from -0.125 to 0.125
- value_weight: bfloat16 [4096, 2048], P('sp', 'tp'), may hold values from -0.09375 to 0.09375
- out_weight: bfloat16 [2048, 4096], P('tp', 'sp'), may hold values from -0.125 to 0.125
- lambdas: float32 [8], P('tp'), may hold values from 0.3 to 0.8
- head_gain: float32 [256], replicated, may hold values from 0.1 to 1.9
Outputs:
- layer_out: bfloat16 [2048, 4096], P(('sp', 'tp'))
Inputs may be any that keep to these rules, and one draw needn't show every extreme that they name: `tokens`: the features' mean changes between 16 equal spans of the sequence.
All inputs are finite; a program needn't handle non-finite values.
Results may differ from a plain program's by a relative error of at most 0.013.
The roundings to bfloat16 on the way count: a program that leaves them out, or rounds other values in their place, can miss the bound.
Values may be sent and summed in bfloat16 or wider, within the bound.
No kernel may reach another device: no remote copies, remote signals or barrier semaphores. Data moves between devices by JAX's collectives and lax.ppermute only.
A program may use at most 128 MiB of HBM per device.

v0:
```python
import jax
import jax.numpy as jnp
from jax import lax
from jax.sharding import PartitionSpec as P

QK = 128
V = 256
ROPE_BASE = 500000.0
EPS_NORM = 0.02


def rotate(values, positions):
    half_dim = values.shape[-1] // 2
    inverse = 1.0 / ROPE_BASE ** (
        jnp.arange(0, 2 * half_dim, 2, dtype=jnp.float32) / (2 * half_dim)
    )
    angles = positions.astype(jnp.float32)[:, None] * inverse[None, :]
    cos_part = jnp.cos(angles)[:, None, :]
    sin_part = jnp.sin(angles)[:, None, :]
    first_half = values[..., :half_dim]
    second_half = values[..., half_dim:]
    return jnp.concatenate(
        [
            first_half * cos_part - second_half * sin_part,
            second_half * cos_part + first_half * sin_part,
        ],
        axis=-1,
    )


def unchanged(carried):
    return carried


def on_device(
    tokens, query_one, query_two, key_one, key_two, value_weight, out_weight, lambdas, head_gain
):
    tp_count = lax.axis_size("tp")
    sp_index = lax.axis_index("sp")
    own_rows = tokens.shape[0]
    local_len = own_rows * tp_count
    half_len = local_len // 2
    heads_here = lambdas.shape[0]
    gathered = lax.all_gather(tokens, "tp", axis=0, tiled=True)
    row_ids = jnp.arange(local_len, dtype=jnp.int32)
    query_pos = sp_index * local_len + row_ids
    pieces = (
        lax.all_gather(query_one, "sp", axis=0, tiled=True),
        lax.all_gather(query_two, "sp", axis=0, tiled=True),
        lax.all_gather(key_one, "sp", axis=0, tiled=True),
        lax.all_gather(key_two, "sp", axis=0, tiled=True),
        lax.all_gather(value_weight, "sp", axis=0, tiled=True),
    )
    projected = tuple(
        (
            jnp.dot(gathered, weight_piece, preferred_element_type=jnp.float32)
            for weight_piece in pieces
        )
    )

    def turned(product):
        return rotate(product.reshape(local_len, heads_here, QK), query_pos).astype(jnp.bfloat16)

    q_one = turned(projected[0])
    q_two = turned(projected[1])
    k_one = turned(projected[2]).reshape(local_len, heads_here * QK)
    k_two = turned(projected[3]).reshape(local_len, heads_here * QK)
    values = projected[4].astype(jnp.bfloat16)
    scale = QK ** (-0.5)
    pieces = (
        lax.all_gather(k_one, "sp", axis=0, tiled=True),
        lax.all_gather(k_two, "sp", axis=0, tiled=True),
        lax.all_gather(values, "sp", axis=0, tiled=True),
    )
    key_count = pieces[0].shape[0]
    global_ids = jnp.arange(key_count, dtype=jnp.int32)
    shard_ids = global_ids // local_len
    within = global_ids % local_len
    key_pos = shard_ids * local_len + within
    key_sets = (
        pieces[0].reshape(key_count, heads_here, QK),
        pieces[1].reshape(key_count, heads_here, QK),
    )
    value_rows = pieces[2].reshape(key_count, heads_here, V)
    row_tops = jnp.full((2, heads_here, local_len), -1e30, jnp.float32)
    totals = jnp.zeros((2, heads_here, local_len), jnp.float32)
    accums = jnp.zeros((2, heads_here, local_len, V), jnp.float32)
    new_parts = []
    for segment in range(2):
        low_row = segment * half_len
        seg_pos = query_pos[low_row : low_row + half_len]
        queries = (q_one[low_row : low_row + half_len], q_two[low_row : low_row + half_len])
        carried = (
            row_tops[:, :, low_row : low_row + half_len],
            totals[:, :, low_row : low_row + half_len],
            accums[:, :, low_row : low_row + half_len],
        )

        def update(carried, queries=queries, seg_pos=seg_pos):
            allowed = key_pos[None, :] <= seg_pos[:, None]
            out_tops, out_totals, out_accums = ([], [], [])
            for map_index in range(2):
                scores = (
                    jnp.einsum(
                        "qhd,khd->hqk",
                        queries[map_index],
                        key_sets[map_index],
                        preferred_element_type=jnp.float32,
                    )
                    * scale
                )
                masked = jnp.where(allowed[None], scores, -1e30)
                old_top = carried[0][map_index]
                new_top = jnp.maximum(old_top, jnp.max(masked, axis=-1))
                exp_weights = jnp.where(allowed[None], jnp.exp(scores - new_top[..., None]), 0.0)
                new_total = jnp.sum(exp_weights, axis=-1)
                new_accum = jnp.einsum(
                    "hqk,khv->hqv",
                    exp_weights.astype(jnp.bfloat16),
                    value_rows,
                    preferred_element_type=jnp.float32,
                )
                out_tops.append(new_top)
                out_totals.append(new_total)
                out_accums.append(new_accum)
            return (jnp.stack(out_tops), jnp.stack(out_totals), jnp.stack(out_accums))

        needed = jnp.min(key_pos) <= jnp.max(seg_pos)
        new_parts.append(lax.cond(needed, update, unchanged, carried))
    row_tops, totals, accums = tuple(
        (
            jnp.concatenate([new_part[member] for new_part in new_parts], axis=2)
            for member in range(3)
        )
    )
    map_outputs = accums / totals[..., None]
    mixed_out = map_outputs[0] - lambdas[:, None, None] * map_outputs[1]
    scaled = (
        mixed_out
        * lax.rsqrt(jnp.mean(mixed_out * mixed_out, axis=-1, keepdims=True) + EPS_NORM)
        * head_gain
    )
    attended = scaled.astype(jnp.bfloat16)
    weight_piece = lax.all_gather(out_weight, "sp", axis=1, tiled=True)
    shaped = weight_piece.reshape(heads_here, V, weight_piece.shape[1])
    partial_terms = jnp.einsum("hqv,hvd->qd", attended, shaped, preferred_element_type=jnp.float32)
    summed = lax.psum_scatter(
        partial_terms.astype(jnp.bfloat16), "tp", scatter_dimension=0, tiled=True
    )
    return summed


def solution(mesh):
    in_specs = (
        P(("sp", "tp"), None),
        P("sp", "tp"),
        P("sp", "tp"),
        P("sp", "tp"),
        P("sp", "tp"),
        P("sp", "tp"),
        P("tp", "sp"),
        P("tp"),
        P(),
    )
    out_specs = P(("sp", "tp"), None)
    return jax.shard_map(
        on_device, mesh=mesh, in_specs=in_specs, out_specs=out_specs, check_vma=False
    )
```

profile of v0, /device:TPU:0, one launch (start us, length us, event | category | flops | bytes accessed | tf_op | source)
XLA Modules:
  0.0 554.6 jit_solution(14938328671323246360)
XLA Ops:
  10.5 23.7 %all-gather.11.cloned.1.call-done = bf16[256,4096]{1,0:T(8,128)(2,1)} async-done(((bf16[64,4096]{1,0:T(8,128)(2,1)}), bf16[256,4096]{1,0:T(8,128)(2,1)}) %all-gather.11.cloned.1.call-update) | async-done | bytes 2097168 | tf_op jit(solution)/shard_map/all_gather | solution.py:44
  34.2 74.9 %all-gather.25.cloned.1.call-done = bf16[4096,512]{1,0:T(8,128)(2,1)} async-done(((bf16[512,512]{1,0:T(8,128)(2,1)}), bf16[4096,512]{1,0:T(8,128)(2,1)}) %all-gather.25.cloned.1.call-update) | async-done | bytes 4194320 | tf_op jit(solution)/shard_map/all_gather | solution.py:52
  109.2 4.8 convolution_convert_fusion
  114.3 44.6 %all-gather.19.cloned.1.call-done = bf16[4096,256]{1,0:T(8,128)(2,1)} async-done(((bf16[512,256]{1,0:T(8,128)(2,1)}), bf16[4096,256]{1,0:T(8,128)(2,1)}) %all-gather.19.cloned.1.call-update) | async-done | bytes 2097168 | tf_op jit(solution)/shard_map/all_gather | solution.py:49
  159.0 2.5 fusion.74
  161.5 47.1 %all-gather.21.cloned.1.call-done = bf16[4096,256]{1,0:T(8,128)(2,1)} async-done(((bf16[512,256]{1,0:T(8,128)(2,1)}), bf16[4096,256]{1,0:T(8,128)(2,1)}) %all-gather.21.cloned.1.call-update) | async-done | bytes 2097168 | tf_op jit(solution)/shard_map/all_gather | solution.py:51
  208.6 2.5 fusion.75
  211.1 47.1 %all-gather.13.cloned.1.call-done = bf16[4096,256]{1,0:T(8,128)(2,1)} async-done(((bf16[512,256]{1,0:T(8,128)(2,1)}), bf16[4096,256]{1,0:T(8,128)(2,1)}) %all-gather.13.cloned.1.call-update) | async-done | bytes 2097168 | tf_op jit(solution)/shard_map/all_gather | solution.py:48
  258.2 2.5 fusion.72
  260.7 47.1 %all-gather.15.cloned.1.call-done = bf16[4096,256]{1,0:T(8,128)(2,1)} async-done(((bf16[512,256]{1,0:T(8,128)(2,1)}), bf16[4096,256]{1,0:T(8,128)(2,1)}) %all-gather.15.cloned.1.call-update) | async-done | bytes 2097168 | tf_op jit(solution)/shard_map/all_gather | solution.py:50
  307.8 2.5 fusion.73
  316.8 40.8 %all-gather.27.cloned.1.call-done = bf16[2048,512]{1,0:T(8,128)(2,1)} async-done(((bf16[256,512]{1,0:T(8,128)(2,1)}), bf16[2048,512]{1,0:T(8,128)(2,1)}) %all-gather.27.cloned.1.call-update) | async-done | bytes 2097168 | tf_op jit(solution)/shard_map/all_gather | solution.py:73
  357.6 4.0 reshape.172
  361.6 36.0 %all-gather.23.cloned.1.call-done = bf16[2048,256]{0,1:T(8,128)(2,1)} async-done(((bf16[256,256]{0,1:T(8,128)(2,1)}), bf16[2048,256]{0,1:T(8,128)(2,1)}) %all-gather.23.cloned.1.call-update) | async-done | bytes 1048592 | tf_op jit(solution)/shard_map/all_gather | solution.py:72
  397.6 40.5 %all-gather.17.cloned.1.call-done = bf16[2048,256]{0,1:T(8,128)(2,1)} async-done(((bf16[256,256]{0,1:T(8,128)(2,1)}), bf16[2048,256]{0,1:T(8,128)(2,1)}) %all-gather.17.cloned.1.call-update) | async-done | bytes 1048592 | tf_op jit(solution)/shard_map/all_gather | solution.py:71
  438.1 8.6 %conditional.2 = (f32[2,2,128]{2,1,0:T(2,128)S(1)}, f32[2,2,128,256]{3,2,1,0:T(8,128)}) conditional(s32[]{:T(128)} %convert_element_type.52, () %tuple.21, (s32[2048]{0:T(1024)S(1)}, s32[128]{0:T(128)S(1)}, bf16[256,2,128]{0,2,1:T(8,128)(2,1)S(1)}, bf16[2048,2,128]{0,2,1:T(8,128)(2,1)}, bf16[256,2,128]{0,2,1:T(8,128)(2,1)S(1)}, ...), branch_computations={%region_2.3_spmd, %region_3.8_spmd} | conditional | flops 815136768 | bytes 35283528 | solution.py:129
  439.1 1.9 select_reduce_fusion.1
  441.8 2.1 fusion.5
  446.7 10.4 %conditional.3 = (f32[2,2,128]{2,1,0:T(2,128)S(1)}, f32[2,2,128,256]{3,2,1,0:T(8,128)}) conditional(s32[]{:T(128)} %convert_element_type.57, () %tuple.23, (s32[2048]{0:T(1024)S(1)}, s32[128]{0:T(128)}, bf16[256,2,128]{0,2,1:T(8,128)(2,1)}, bf16[2048,2,128]{0,2,1:T(8,128)(2,1)}, bf16[256,2,128]{0,2,1:T(8,128)(2,1)S(1)}, ...), branch_computations={%region_9.10_spmd, %region_10.15_spmd} | conditional | flops 815136768 | bytes 35283528 | solution.py:129
  449.5 1.9 select_reduce_fusion.3
  452.2 2.1 fusion.31
  458.8 54.9 %all-gather.29.cloned.1.call-done = bf16[512,4096]{1,0:T(8,128)(2,1)} async-done(((bf16[512,512]{1,0:T(8,128)(2,1)}), bf16[512,4096]{1,0:T(8,128)(2,1)}) %all-gather.29.cloned.1.call-update) | async-done | bytes 4194320 | tf_op jit(solution)/shard_map/all_gather | solution.py:144
  513.7 4.8 fusion.52
  518.5 29.5 %reduce-scatter.2.cloned.1.call-done = bf16[64,4096]{1,0:T(8,128)(2,1)} async-done(((bf16[256,4096]{1,0:T(8,128)(2,1)}), bf16[64,4096]{1,0:T(8,128)(2,1)}) %reduce-scatter.2.cloned.1.call-update) | async-done | bytes 524304 | tf_op jit(solution)/shard_map/reduce_scatter | solution.py:147
  (73 shorter events, 20.7 us)
Async XLA Ops:
  6.5 27.7 %all-gather.11.cloned.1.call-start = ((), (), s32[]{:S(2)}) async-start(), calls=%async_computation.1 | async-start | bytes 2621440 | tf_op jit(solution)/shard_map/all_gather | solution.py:44
  7.3 101.9 %all-gather.25.cloned.1.call-start = ((), (), s32[]{:S(2)}) async-start(), calls=%async_computation.8 | async-start | bytes 4718592 | tf_op jit(solution)/shard_map/all_gather | solution.py:52
  8.0 150.9 %all-gather.19.cloned.1.call-start = ((), (), s32[]{:S(2)}) async-start(), calls=%async_computation.5 | async-start | bytes 2359296 | tf_op jit(solution)/shard_map/all_gather | solution.py:49
  8.7 199.9 %all-gather.21.cloned.1.call-start = ((), (), s32[]{:S(2)}) async-start(), calls=%async_computation.6 | async-start | bytes 2359296 | tf_op jit(solution)/shard_map/all_gather | solution.py:51
  9.3 248.9 %all-gather.13.cloned.1.call-start = ((), (), s32[]{:S(2)}) async-start(), calls=%async_computation.2 | async-start | bytes 2359296 | tf_op jit(solution)/shard_map/all_gather | solution.py:48
  9.9 297.9 %all-gather.15.cloned.1.call-start = ((), (), s32[]{:S(2)}) async-start(), calls=%async_computation.3 | async-start | bytes 2359296 | tf_op jit(solution)/shard_map/all_gather | solution.py:50
  10.5 347.1 %all-gather.27.cloned.1.call-start = ((), (), s32[]{:S(2)}) async-start(), calls=%async_computation.9 | async-start | bytes 2359296 | tf_op jit(solution)/shard_map/all_gather | solution.py:73
  34.2 124.7 %copy-start = (bf16[256,4096]{1,0:T(8,128)(2,1)S(1)}, bf16[256,4096]{1,0:T(8,128)(2,1)}, u32[]{:S(2)}) copy-start(bf16[256,4096]{1,0:T(8,128)(2,1)} %all-gather.11.cloned.1.call-done) | copy-start | bytes 6291460
  114.0 283.7 %all-gather.23.cloned.1.call-start = ((), (), s32[]{:S(2)}) async-start(), calls=%async_computation.7 | async-start | bytes 1179648 | tf_op jit(solution)/shard_map/all_gather | solution.py:72
  311.2 126.9 %all-gather.17.cloned.1.call-start = ((), (), s32[]{:S(2)}) async-start(), calls=%async_computation.4 | async-start | bytes 1179648 | tf_op jit(solution)/shard_map/all_gather | solution.py:71
  312.0 201.7 %all-gather.29.cloned.1.call-start = ((), (), s32[]{:S(2)}) async-start(), calls=%async_computation.10 | async-start | bytes 4718592 | tf_op jit(solution)/shard_map/all_gather | solution.py:144
  312.5 235.5 %reduce-scatter.2.cloned.1.call-start = ((), (), s32[]{:S(2)}) async-start(), calls=%async_computation.11 | async-start | bytes 2621440 | tf_op jit(solution)/shard_map/reduce_scatter | solution.py:147
  316.8 121.3 %copy-start.5 = (bf16[256,2,128]{0,2,1:T(8,128)(2,1)}, bf16[256,2,128]{0,2,1:T(8,128)(2,1)S(1)}, u32[]{:S(2)}) copy-start(bf16[256,2,128]{0,2,1:T(8,128)(2,1)S(1)} %pad_maximum_fusion.4) | copy-start | bytes 393220
  438.1 3.7 copy-start.1
  441.8 2.1 copy-start.3
  446.9 5.3 copy-start.2
  452.2 2.1 copy-start.4
  457.1 1.5 copy-start.6
  457.1 56.6 %copy-start.7 = (f32[256]{0:T(256)S(1)}, f32[256]{0:T(256)}, u32[]{:S(2)}) copy-start(f32[256]{0:T(256)} %param.21) | copy-start | bytes 3076
Sparse Core Ops, SparseCore 0:
  8.9 25.2 all-gather.10
  36.3 72.7 all-gather.24
  111.3 47.6 all-gather.18
  160.9 47.6 all-gather.20
  210.6 47.5 all-gather.12
  260.2 47.6 all-gather.14
  310.0 47.6 all-gather.26
  359.7 37.9 all-gather.22
  399.7 38.3 all-gather.16
  440.0 73.6 all-gather.28
  518.7 29.3 reduce-scatter.1
where the time goes:
time: 555 us
  waiting for transfers between devices  490 us (88%)
  matrix products  30.4 us (5%)
  between operations  15.7 us (3%)
  other arithmetic  9.28 us (2%)
  local copies, waits for them, and re-layouts  7.99 us (1%)
    all_gather x1, waiting for transfers between devices, on_device(): lax.all_gather(value_weight, 'sp', axis=0, tiled=True)  74.9 us
    all_gather x1, waiting for transfers between devices, on_device(): weight_piece = lax.all_gather(out_weight, 'sp', axis=1, tiled=True)  54.9 us
    all_gather x1, waiting for transfers between devices, on_device(): lax.all_gather(key_two, 'sp', axis=0, tiled=True)  47.1 us
    all_gather x1, waiting for transfers between devices, on_device(): lax.all_gather(key_one, 'sp', axis=0, tiled=True)  47.1 us
    all_gather x1, waiting for transfers between devices, on_device(): lax.all_gather(query_one, 'sp', axis=0, tiled=True)  47.1 us
    all_gather x1, waiting for transfers between devices, on_device(): lax.all_gather(query_two, 'sp', axis=0, tiled=True)  44.6 us
    all_gather x1, waiting for transfers between devices, on_device(): lax.all_gather(values, 'sp', axis=0, tiled=True)  40.8 us
    all_gather x1, waiting for transfers between devices, on_device(): lax.all_gather(k_one, 'sp', axis=0, tiled=True)  40.5 us
  transfers between devices with their start and end apart: 11, of which 11 were waited for; matrix products, arithmetic and copies ran while one was open for 8% of the time, Pallas kernels for 0%

commit v1 on v0

--- a/solution.py
+++ b/solution.py
@@ -7,6 +7,27 @@
 V = 256
 ROPE_BASE = 500000.0
 EPS_NORM = 0.02
+
+
+def gather_around(x, axis, dim):
+    peers, index, span = (lax.axis_size(axis), lax.axis_index(axis), x.shape[dim])
+    right = [(i, (i + 1) % peers) for i in range(peers)]
+    behind = [(i, (i - 1) % peers) for i in range(peers)]
+    filled = jnp.zeros((*x.shape[:dim], peers * span, *x.shape[dim + 1 :]), x.dtype)
+    filled = lax.dynamic_update_slice_in_dim(filled, x, index * span, axis=dim)
+    from_left = from_right = x
+    half = peers // 2
+    for step in range(1, half + 1):
+        from_left = lax.ppermute(from_left, axis, right)
+        filled = lax.dynamic_update_slice_in_dim(
+            filled, from_left, (index - step) % peers * span, axis=dim
+        )
+        if step < peers - half:
+            from_right = lax.ppermute(from_right, axis, behind)
+            filled = lax.dynamic_update_slice_in_dim(
+                filled, from_right, (index + step) % peers * span, axis=dim
+            )
+    return filled
 
 
 def rotate(values, positions):
@@ -48,7 +69,7 @@
         lax.all_gather(query_one, "sp", axis=0, tiled=True),
         lax.all_gather(query_two, "sp", axis=0, tiled=True),
         lax.all_gather(key_one, "sp", axis=0, tiled=True),
-        lax.all_gather(key_two, "sp", axis=0, tiled=True),
+        gather_around(key_two, "sp", 0),
         lax.all_gather(value_weight, "sp", axis=0, tiled=True),
     )
     projected = tuple(

time: 555 us -> 528 us (0.951)
  waiting for transfers between devices: 490 us -> 439 us
  starting transfers between devices: 0.39 us -> 16.8 us
  local copies, waits for them, and re-layouts: 7.99 us -> 15.2 us
    all_gather x1 -> x0, waiting for transfers between devices: 47.1 us -> none  [on_device(): lax.all_gather(key_two, 'sp', axis=0, tiled=True)]
    all_gather x1, waiting for transfers between devices: 44.6 us -> 6.41 us  [on_device(): lax.all_gather(query_two, 'sp', axis=0, tiled=True)]
    ppermute x0 -> x7, waiting for transfers between devices: none -> 32.8 us  [the longest x4 27.8 us: gather_around(): from_left = lax.ppermute(from_left, axis, right)]
    ppermute x0 -> x7, starting transfers between devices: none -> 16.4 us  [the longest x3 8.38 us: gather_around(): from_right = lax.ppermute(from_right, axis, behind)]
    dynamic_update_slice x0 -> x8, local copies, waits for them, and re-layouts: none -> 5.76 us  [the longest x4 2.92 us: gather_around(): lax.dynamic_update_slice_in_dim(filled, from_left, (index - step) % peers...]
  transfers between devices with their start and end apart: 11 -> 17, of which waited for: 11 -> 17; matrix products, arithmetic and copies ran while one was open for 8% -> 9% of each run, Pallas kernels for 0% -> 0%
where the time goes in v1:
time: 528 us; the launch traced here: 527 us
  waiting for transfers between devices  439 us (83%)
  matrix products  30.3 us (6%)
  starting transfers between devices  16.8 us (3%)
  between operations  16.2 us (3%)
  local copies, waits for them, and re-layouts  15.2 us (3%)
  other arithmetic  9.2 us (2%)
    all_gather x1, waiting for transfers between devices, on_device(): lax.all_gather(value_weight, 'sp', axis=0, tiled=True)  75 us
    all_gather x1, waiting for transfers between devices, on_device(): weight_piece = lax.all_gather(out_weight, 'sp', axis=1, tiled=True)  55.8 us
    all_gather x1, waiting for transfers between devices, on_device(): lax.all_gather(query_one, 'sp', axis=0, tiled=True)  47.4 us
    all_gather x1, waiting for transfers between devices, on_device(): lax.all_gather(key_one, 'sp', axis=0, tiled=True)  47.1 us
    all_gather x1, waiting for transfers between devices, on_device(): lax.all_gather(k_one, 'sp', axis=0, tiled=True)  40.5 us
    all_gather x1, waiting for transfers between devices, on_device(): lax.all_gather(values, 'sp', axis=0, tiled=True)  40.4 us
    all_gather x1, waiting for transfers between devices, on_device(): lax.all_gather(k_two, 'sp', axis=0, tiled=True)  36 us
    reduce_scatter x1, waiting for transfers between devices, on_device(): lax.psum_scatter(partial_terms.astype(jnp.bfloat16), 'tp', scatter_dimens...  29.5 us
  transfers between devices with their start and end apart: 17, of which 17 were waited for; matrix products, arithmetic and copies ran while one was open for 9% of the time, Pallas kernels for 0%

profile of v1, /device:TPU:0, one launch (start us, length us, event | category | flops | bytes accessed | tf_op | source)
XLA Modules:
  0.0 527.0 jit_solution(6882979670573635744)
XLA Ops:
  10.0 24.2 %all-gather.10.cloned.1.call-done = bf16[256,4096]{1,0:T(8,128)(2,1)} async-done(((bf16[64,4096]{1,0:T(8,128)(2,1)}), bf16[256,4096]{1,0:T(8,128)(2,1)}) %all-gather.10.cloned.1.call-update) | async-done | bytes 2097168 | tf_op jit(solution)/shard_map/all_gather | solution.py:65
  34.2 75.0 %all-gather.22.cloned.1.call-done = bf16[4096,512]{1,0:T(8,128)(2,1)} async-done(((bf16[512,512]{1,0:T(8,128)(2,1)}), bf16[4096,512]{1,0:T(8,128)(2,1)}) %all-gather.22.cloned.1.call-update) | async-done | bytes 4194320 | tf_op jit(solution)/shard_map/all_gather | solution.py:73
  109.2 4.8 convolution_convert_fusion
  114.6 4.2 collective-permute-start.1
  118.8 10.4 %collective-permute-done = bf16[512,256]{1,0:T(8,128)(2,1)S(1)} collective-permute-done((bf16[512,256]{1,0:T(8,128)(2,1)S(1)}, bf16[512,256]{1,0:T(8,128)(2,1)S(1)}, u32[]{:S(2)}, u32[]{:S(2)}) %collective-permute-start) | collective-permute-done | bytes 262176 | tf_op jit(solution)/shard_map/ppermute | solution.py:21
  136.6 5.3 %collective-permute-done.2 = bf16[512,256]{1,0:T(8,128)(2,1)S(1)} collective-permute-done((bf16[512,256]{1,0:T(8,128)(2,1)S(1)}, bf16[512,256]{1,0:T(8,128)(2,1)S(1)}, u32[]{:S(2)}, u32[]{:S(2)}) %collective-permute-start.2) | collective-permute-done | bytes 262176 | tf_op jit(solution)/shard_map/ppermute | solution.py:21
  148.2 3.9 collective-permute-start.5
  152.9 7.9 %collective-permute-done.4 = bf16[512,256]{1,0:T(8,128)(2,1)S(1)} collective-permute-done((bf16[512,256]{1,0:T(8,128)(2,1)S(1)}, bf16[512,256]{1,0:T(8,128)(2,1)S(1)}, u32[]{:S(2)}, u32[]{:S(2)}) %collective-permute-start.4) | collective-permute-done | bytes 262176 | tf_op jit(solution)/shard_map/ppermute | solution.py:21
  165.9 4.2 collective-permute-done.6
  173.2 6.4 %all-gather.18.cloned.1.call-done = bf16[4096,256]{1,0:T(8,128)(2,1)} async-done(((bf16[512,256]{1,0:T(8,128)(2,1)}), bf16[4096,256]{1,0:T(8,128)(2,1)}) %all-gather.18.cloned.1.call-update) | async-done | bytes 2097168 | tf_op jit(solution)/shard_map/all_gather | solution.py:70
  179.6 2.5 fusion.74
  182.2 47.4 %all-gather.12.cloned.1.call-done = bf16[4096,256]{1,0:T(8,128)(2,1)} async-done(((bf16[512,256]{1,0:T(8,128)(2,1)}), bf16[4096,256]{1,0:T(8,128)(2,1)}) %all-gather.12.cloned.1.call-update) | async-done | bytes 2097168 | tf_op jit(solution)/shard_map/all_gather | solution.py:69
  229.6 2.5 fusion.72
  232.1 47.1 %all-gather.14.cloned.1.call-done = bf16[4096,256]{1,0:T(8,128)(2,1)} async-done(((bf16[512,256]{1,0:T(8,128)(2,1)}), bf16[4096,256]{1,0:T(8,128)(2,1)}) %all-gather.14.cloned.1.call-update) | async-done | bytes 2097168 | tf_op jit(solution)/shard_map/all_gather | solution.py:71
  279.2 2.5 fusion.73
  288.5 40.4 %all-gather.24.cloned.1.call-done = bf16[2048,512]{1,0:T(8,128)(2,1)} async-done(((bf16[256,512]{1,0:T(8,128)(2,1)}), bf16[2048,512]{1,0:T(8,128)(2,1)}) %all-gather.24.cloned.1.call-update) | async-done | bytes 2097168 | tf_op jit(solution)/shard_map/all_gather | solution.py:94
  328.9 4.0 reshape.172
  332.9 36.0 %all-gather.20.cloned.1.call-done = bf16[2048,256]{0,1:T(8,128)(2,1)} async-done(((bf16[256,256]{0,1:T(8,128)(2,1)}), bf16[2048,256]{0,1:T(8,128)(2,1)}) %all-gather.20.cloned.1.call-update) | async-done | bytes 1048592 | tf_op jit(solution)/shard_map/all_gather | solution.py:93
  368.9 40.5 %all-gather.16.cloned.1.call-done = bf16[2048,256]{0,1:T(8,128)(2,1)} async-done(((bf16[256,256]{0,1:T(8,128)(2,1)}), bf16[2048,256]{0,1:T(8,128)(2,1)}) %all-gather.16.cloned.1.call-update) | async-done | bytes 1048592 | tf_op jit(solution)/shard_map/all_gather | solution.py:92
  409.4 8.6 %conditional.2 = (f32[2,2,128]{2,1,0:T(2,128)S(1)}, f32[2,2,128,256]{3,2,1,0:T(8,128)}) conditional(s32[]{:T(128)} %convert_element_type.52, () %tuple.21, (s32[2048]{0:T(1024)S(1)}, s32[128]{0:T(128)S(1)}, bf16[256,2,128]{0,2,1:T(8,128)(2,1)S(1)}, bf16[2048,2,128]{0,2,1:T(8,128)(2,1)}, bf16[256,2,128]{0,2,1:T(8,128)(2,1)S(1)}, ...), branch_computations={%region_2.3_spmd, %region_3.8_spmd} | conditional | flops 815136768 | bytes 35283528 | solution.py:150
  417.9 10.4 %conditional.3 = (f32[2,2,128]{2,1,0:T(2,128)S(1)}, f32[2,2,128,256]{3,2,1,0:T(8,128)}) conditional(s32[]{:T(128)} %convert_element_type.57, () %tuple.23, (s32[2048]{0:T(1024)S(1)}, s32[128]{0:T(128)}, bf16[256,2,128]{0,2,1:T(8,128)(2,1)}, bf16[2048,2,128]{0,2,1:T(8,128)(2,1)}, bf16[256,2,128]{0,2,1:T(8,128)(2,1)S(1)}, ...), branch_computations={%region_9.10_spmd, %region_10.15_spmd} | conditional | flops 815136768 | bytes 35283528 | solution.py:150
  430.0 55.8 %all-gather.26.cloned.1.call-done = bf16[512,4096]{1,0:T(8,128)(2,1)} async-done(((bf16[512,512]{1,0:T(8,128)(2,1)}), bf16[512,4096]{1,0:T(8,128)(2,1)}) %all-gather.26.cloned.1.call-update) | async-done | bytes 4194320 | tf_op jit(solution)/shard_map/all_gather | solution.py:165
  485.8 4.8 fusion.52
  490.7 29.5 %reduce-scatter.2.cloned.1.call-done = bf16[64,4096]{1,0:T(8,128)(2,1)} async-done(((bf16[256,4096]{1,0:T(8,128)(2,1)}), bf16[64,4096]{1,0:T(8,128)(2,1)}) %reduce-scatter.2.cloned.1.call-update) | async-done | bytes 524304 | tf_op jit(solution)/shard_map/reduce_scatter | solution.py:168
  (95 shorter events, 51.2 us)
Async XLA Ops:
  6.5 27.7 %all-gather.10.cloned.1.call-start = ((), (), s32[]{:S(2)}) async-start(), calls=%async_computation.1 | async-start | bytes 2621440 | tf_op jit(solution)/shard_map/all_gather | solution.py:65
  7.3 101.9 %all-gather.22.cloned.1.call-start = ((), (), s32[]{:S(2)}) async-start(), calls=%async_computation.7 | async-start | bytes 4718592 | tf_op jit(solution)/shard_map/all_gather | solution.py:73
  8.0 171.6 %all-gather.18.cloned.1.call-start = ((), (), s32[]{:S(2)}) async-start(), calls=%async_computation.5 | async-start | bytes 2359296 | tf_op jit(solution)/shard_map/all_gather | solution.py:70
  8.7 220.9 %all-gather.12.cloned.1.call-start = ((), (), s32[]{:S(2)}) async-start(), calls=%async_computation.2 | async-start | bytes 2359296 | tf_op jit(solution)/shard_map/all_gather | solution.py:69
  9.3 269.9 %all-gather.14.cloned.1.call-start = ((), (), s32[]{:S(2)}) async-start(), calls=%async_computation.3 | async-start | bytes 2359296 | tf_op jit(solution)/shard_map/all_gather | solution.py:71
  9.9 104.1 %copy-start.6 = (bf16[512,256]{1,0:T(8,128)(2,1)S(1)}, bf16[512,256]{1,0:T(8,128)(2,1)}, u32[]{:S(2)}) copy-start(bf16[512,256]{1,0:T(8,128)(2,1)} %param.17) | copy-start | bytes 786436
  9.9 319.0 %all-gather.24.cloned.1.call-start = ((), (), s32[]{:S(2)}) async-start(), calls=%async_computation.8 | async-start | bytes 2359296 | tf_op jit(solution)/shard_map/all_gather | solution.py:94
  114.0 254.9 %all-gather.20.cloned.1.call-start = ((), (), s32[]{:S(2)}) async-start(), calls=%async_computation.6 | async-start | bytes 1179648 | tf_op jit(solution)/shard_map/all_gather | solution.py:93
  114.0 15.2 %collective-permute-start = (bf16[512,256]{1,0:T(8,128)(2,1)S(1)}, bf16[512,256]{1,0:T(8,128)(2,1)S(1)}, u32[]{:S(2)}, u32[]{:S(2)}) collective-permute-start(bf16[512,256]{1,0:T(8,128)(2,1)S(1)} %copy-done.6), channel_id=1, source_target_pairs={{0,4},{4,8},{8,12},{12,16},{16,20},{20,24},{24,28},{28,0},{1,5},{5... | collective-permute-start | bytes 786440 | tf_op jit(solution)/shard_map/ppermute | solution.py:21
  114.6 19.5 %collective-permute-start.1 = (bf16[512,256]{1,0:T(8,128)(2,1)S(1)}, bf16[512,256]{1,0:T(8,128)(2,1)S(1)}, u32[]{:S(2)}, u32[]{:S(2)}) collective-permute-start(bf16[512,256]{1,0:T(8,128)(2,1)S(1)} %copy-done.6), channel_id=1, source_target_pairs={{0,28},{4,0},{8,4},{12,8},{16,12},{20,16},{24,20},{28,24},{1,29},{... | collective-permute-start | bytes 786440 | tf_op jit(solution)/shard_map/ppermute | solution.py:26
  129.2 12.7 %collective-permute-start.2 = (bf16[512,256]{1,0:T(8,128)(2,1)S(1)}, bf16[512,256]{1,0:T(8,128)(2,1)S(1)}, u32[]{:S(2)}, u32[]{:S(2)}) collective-permute-start(bf16[512,256]{1,0:T(8,128)(2,1)S(1)} %collective-permute-done), channel_id=1, source_target_pairs={{0,4},{4,8},{8,12},{12,16},{16,20},{20,24},{24,28},{28,0},{1,5},{5... | collective-permute-start | bytes 786440 | tf_op jit(solution)/shard_map/ppermute | solution.py:21
  134.2 14.1 %collective-permute-start.3 = (bf16[512,256]{1,0:T(8,128)(2,1)S(1)}, bf16[512,256]{1,0:T(8,128)(2,1)S(1)}, u32[]{:S(2)}, u32[]{:S(2)}) collective-permute-start(bf16[512,256]{1,0:T(8,128)(2,1)S(1)} %collective-permute-done.1), channel_id=1, source_target_pairs={{0,28},{4,0},{8,4},{12,8},{16,12},{20,16},{24,20},{28,24},{1,29},{... | collective-permute-start | bytes 786440 | tf_op jit(solution)/shard_map/ppermute | solution.py:26
  135.9 34.9 %copy-start = (bf16[256,4096]{1,0:T(8,128)(2,1)S(1)}, bf16[256,4096]{1,0:T(8,128)(2,1)}, u32[]{:S(2)}) copy-start(bf16[256,4096]{1,0:T(8,128)(2,1)} %all-gather.10.cloned.1.call-done) | copy-start | bytes 6291460
  141.9 18.9 %collective-permute-start.4 = (bf16[512,256]{1,0:T(8,128)(2,1)S(1)}, bf16[512,256]{1,0:T(8,128)(2,1)S(1)}, u32[]{:S(2)}, u32[]{:S(2)}) collective-permute-start(bf16[512,256]{1,0:T(8,128)(2,1)S(1)} %collective-permute-done.2), channel_id=1, source_target_pairs={{0,4},{4,8},{8,12},{12,16},{16,20},{20,24},{24,28},{28,0},{1,5},{5... | collective-permute-start | bytes 786440 | tf_op jit(solution)/shard_map/ppermute | solution.py:21
  148.2 17.0 %collective-permute-start.5 = (bf16[512,256]{1,0:T(8,128)(2,1)S(1)}, bf16[512,256]{1,0:T(8,128)(2,1)S(1)}, u32[]{:S(2)}, u32[]{:S(2)}) collective-permute-start(bf16[512,256]{1,0:T(8,128)(2,1)S(1)} %collective-permute-done.3), channel_id=1, source_target_pairs={{0,28},{4,0},{8,4},{12,8},{16,12},{20,16},{24,20},{28,24},{1,29},{... | collective-permute-start | bytes 786440 | tf_op jit(solution)/shard_map/ppermute | solution.py:26
  160.8 9.3 %collective-permute-start.6 = (bf16[512,256]{1,0:T(8,128)(2,1)S(1)}, bf16[512,256]{1,0:T(8,128)(2,1)S(1)}, u32[]{:S(2)}, u32[]{:S(2)}) collective-permute-start(bf16[512,256]{1,0:T(8,128)(2,1)S(1)} %collective-permute-done.4), channel_id=1, source_target_pairs={{0,4},{4,8},{8,12},{12,16},{16,20},{20,24},{24,28},{28,0},{1,5},{5... | collective-permute-start | bytes 786440 | tf_op jit(solution)/shard_map/ppermute | solution.py:21
  282.6 126.8 %all-gather.16.cloned.1.call-start = ((), (), s32[]{:S(2)}) async-start(), calls=%async_computation.4 | async-start | bytes 1179648 | tf_op jit(solution)/shard_map/all_gather | solution.py:92
  283.3 202.5 %all-gather.26.cloned.1.call-start = ((), (), s32[]{:S(2)}) async-start(), calls=%async_computation.9 | async-start | bytes 4718592 | tf_op jit(solution)/shard_map/all_gather | solution.py:165
  284.1 236.1 %reduce-scatter.2.cloned.1.call-start = ((), (), s32[]{:S(2)}) async-start(), calls=%async_computation.10 | async-start | bytes 2621440 | tf_op jit(solution)/shard_map/reduce_scatter | solution.py:168
  288.5 120.9 %copy-start.5 = (bf16[256,2,128]{0,2,1:T(8,128)(2,1)}, bf16[256,2,128]{0,2,1:T(8,128)(2,1)S(1)}, u32[]{:S(2)}) copy-start(bf16[256,2,128]{0,2,1:T(8,128)(2,1)S(1)} %pad_maximum_fusion.4) | copy-start | bytes 393220
  409.4 3.7 copy-start.1
  418.1 5.3 %copy-start.2 = (bf16[2048,2,128]{0,2,1:T(8,128)(2,1)S(1)}, bf16[2048,2,128]{0,2,1:T(8,128)(2,1)}, u32[]{:S(2)}) copy-start(bf16[2048,2,128]{0,2,1:T(8,128)(2,1)} %get-tuple-element.85) | copy-start | bytes 3145732 | tf_op jit(solution)/shard_map/cond
  423.4 2.1 copy-start.4
  428.3 57.5 %copy-start.8 = (f32[256]{0:T(256)S(1)}, f32[256]{0:T(256)}, u32[]{:S(2)}) copy-start(f32[256]{0:T(256)} %param.21) | copy-start | bytes 3076
  (2 other events, 3.5 us)
Sparse Core Ops, SparseCore 0:
  8.9 25.2 all-gather.9
  36.3 72.7 all-gather.21
  111.3 68.3 all-gather.17
  181.6 47.9 all-gather.11
  231.6 47.6 all-gather.13
  281.2 47.6 all-gather.23
  330.9 37.9 all-gather.19
  370.9 38.3 all-gather.15
  411.4 74.3 all-gather.25
  490.8 29.3 reduce-scatter.1
